TPU v7x, 256 devices: a 4x2x16 block of a 4x16x16 slice. The times are simulated.
256 devices in a mesh: grp: 2 (over y), fs: 32 (over z, core), tp: 4 (over x).
Axes of the slice: x: 4, y: 2, z: 16, core: 2. Of those that a mesh axis runs over, the one named last changes fastest.
The devices are a block of a 4x16x16 slice.
Arguments:
- prompt: bfloat16 [8, 1024, 2048], P(('grp', 'tp')), parts along dimension 0, may hold values from -6 to 6
- gate_first: float32 [2048, 5632], P('fs', 'tp'), may hold values from -0.125 to 0.125
- up_first: float32 [2048, 5632], P('fs', 'tp'), may hold values from -0.125 to 0.125
- down_first: float32 [5632, 2048], P('fs', 'tp'), may hold values from -0.3125 to 0.3125
- norm_gain: float32 [2048], replicated, may hold values from 0.1 to 1.9
- gate_second: float32 [2048, 5632], P('fs', 'tp'), may hold values from -0.125 to 0.125
- up_second: float32 [2048, 5632], P('fs', 'tp'), may hold values from -0.125 to 0.125
- down_second: float32 [5632, 2048], P('fs', 'tp'), may hold values from -0.3125 to 0.3125
Outputs:
- result: bfloat16 [8, 1024, 2048], P(('grp', 'tp'), 'fs'), parts along dimension 0
- gate_one: bfloat16 [4096, 5632], P('grp', 'fs'), parts along dimension 0
- up_one: bfloat16 [4096, 5632], P('grp', 'fs'), parts along dimension 0
- down_one: bfloat16 [5632, 4096], P('fs', 'grp'), parts along dimension 1
- gate_two: bfloat16 [4096, 5632], P('grp', 'fs'), parts along dimension 0
- up_two: bfloat16 [4096, 5632], P('grp', 'fs'), parts along dimension 0
- down_two: bfloat16 [5632, 4096], P('fs', 'grp'), parts along dimension 1
There are 2 independent parts, one for each index of `grp`. A program takes and returns all parts, laid end to end along the dimension named above; an argument that names none is the same for every part. Nothing has to cross between parts.
All inputs are finite; a program needn't handle non-finite values.
Results may differ from a plain program's by a relative error of at most 0.029.
Values may be sent and summed in bfloat16 or wider, within the bound.
A program may use at most 64 MiB of HBM per device.

v0:
```python
import jax
import jax.numpy as jnp
from jax import lax
from jax.sharding import Mesh
from jax.sharding import PartitionSpec as P

FS = ("fs_0", "fs_1")
norm_eps = 1e-05
deep_alpha = 2.0**0.25
half_step = 0.5


def reduced_to_own(pieces, axes, sequence):
    inside = pieces.shape[1:]
    pieces = pieces.reshape(*(lax.axis_size(a) for a in axes), *inside)
    pieces = jnp.moveaxis(pieces, sequence, range(len(axes))).reshape(-1, *inside)
    for k in sequence:
        pieces = lax.psum_scatter(pieces, axes[k], scatter_dimension=0, tiled=True)
    return pieces[0]


def cut_along(value, dim, size):
    before, after = (value.shape[:dim], value.shape[dim + 1 :])
    return jnp.moveaxis(value.reshape(*before, size, -1, *after), dim, 0)


def scatter_axes(value, axes, sequence, dim):
    size = lax.axis_size(axes)
    return reduced_to_own(cut_along(value, dim, size), axes, sequence)


def plain_norm(values):
    row_mean = jnp.mean(values, axis=-1, keepdims=True)
    centred = values - row_mean
    variance = jnp.mean(centred * centred, axis=-1, keepdims=True)
    return centred * lax.rsqrt(variance + norm_eps)


def gated_hidden(inputs, gate_proj, up_proj):
    gate_act = jnp.dot(inputs, gate_proj, preferred_element_type=jnp.float32)
    up_act = jnp.dot(inputs, up_proj, preferred_element_type=jnp.float32)
    return (jax.nn.silu(gate_act) * up_act).astype(jnp.bfloat16)


def relay_weights(gate_proj, up_proj, down_proj):
    gate_rows, up_rows, down_mine = (
        lax.all_gather(gate_proj, "tp", axis=1, tiled=True),
        lax.all_gather(up_proj, "tp", axis=1, tiled=True),
        lax.all_gather(down_proj, "tp", axis=1, tiled=True),
    )
    gate_mine, up_mine = (
        lax.all_to_all(gate_rows, FS, split_axis=1, concat_axis=0, tiled=True),
        lax.all_to_all(up_rows, FS, split_axis=1, concat_axis=0, tiled=True),
    )
    return (gate_mine, up_mine, down_mine)


def row_terms(hidden, down_proj):
    return jnp.dot(hidden, down_proj, preferred_element_type=jnp.float32)


def body(prompt, gate_first, up_first, down_first, norm_gain, gate_second, up_second, down_second):
    fs_index = lax.axis_index(FS)
    row_block = gate_first.shape[0]
    gain_rows = lax.dynamic_slice_in_dim(norm_gain, fs_index * row_block, row_block, 0)
    gate_one, up_one, down_one = relay_weights(
        gate_first.astype(jnp.bfloat16),
        up_first.astype(jnp.bfloat16),
        down_first.astype(jnp.bfloat16),
    )
    gate_two, up_two, down_two = relay_weights(
        (gain_rows[:, None] * gate_second).astype(jnp.bfloat16),
        (gain_rows[:, None] * up_second).astype(jnp.bfloat16),
        down_second.astype(jnp.bfloat16),
    )
    tokens = prompt.reshape(-1, prompt.shape[-1])
    own_count = tokens.shape[0] // lax.axis_size(FS)
    own_first = fs_index * own_count
    hidden_one = gated_hidden(tokens, gate_one, up_one)
    own_tokens = lax.dynamic_slice_in_dim(tokens, own_first, own_count, 0)
    ffn_one = scatter_axes(
        row_terms(hidden_one, down_one).astype(jnp.bfloat16), FS, (1, 0), 0
    ).astype(jnp.float32)
    normed_own = plain_norm(
        deep_alpha * own_tokens.astype(jnp.float32) + half_step * ffn_one
    ).astype(jnp.bfloat16)
    hidden_two = gated_hidden(lax.all_gather(normed_own, FS, axis=0, tiled=True), gate_two, up_two)
    ffn_two = scatter_axes(
        row_terms(hidden_two, down_two).astype(jnp.bfloat16), FS, (1, 0), 0
    ).astype(jnp.float32)
    residual_two = deep_alpha * norm_gain * normed_own.astype(jnp.float32)
    result = plain_norm(residual_two + half_step * ffn_two).astype(jnp.bfloat16)
    return (
        result.reshape(1, result.shape[0], result.shape[-1]),
        gate_one,
        up_one,
        down_one,
        gate_two,
        up_two,
        down_two,
    )


def solution(mesh):
    torus = Mesh(
        mesh.devices.reshape(mesh.shape["grp"], 16, 2, mesh.shape["tp"]),
        ("grp", "fs_0", "fs_1", "tp"),
    )
    placed = (
        P(("grp", "tp"), None, None),
        P(FS, "tp"),
        P(FS, "tp"),
        P(FS, "tp"),
        P(),
        P(FS, "tp"),
        P(FS, "tp"),
        P(FS, "tp"),
    )
    return jax.shard_map(
        body,
        mesh=torus,
        in_specs=placed,
        out_specs=(
            P(("grp", "tp"), FS, None),
            P("grp", FS),
            P("grp", FS),
            P(FS, "grp"),
            P("grp", FS),
            P("grp", FS),
            P(FS, "grp"),
        ),
        check_vma=False,
    )
```

profile of v0, /device:TPU:34, one launch (start us, length us, event | category | flops | bytes accessed | tf_op | source)
XLA Modules:
  0.0 540.0 jit_solution(11706451847986128299)
XLA Ops:
  8.2 29.5 %all_gather.21 = bf16[64,5632]{1,0:T(8,128)(2,1)S(1)} all-gather(bf16[64,1408]{1,0:T(8,128)(2,1)S(1)} %convert_element_type.62), channel_id=1, replica_groups=mesh['grp'=2,'fs_0'=16,'fs_1'=2,'tp'=4] {'tp'}, dimensions={1}, use_global_device_ids=true | all-gather | bytes 901120 | tf_op jit(solution)/shard_map/all_gather | solution.py:47
  41.4 9.7 %all-to-all-start = ((bf16[64,32,176]{2,0,1:T(8,128)(2,1)}), bf16[64,32,176]{2,0,1:T(8,128)(2,1)S(1)}, u32[]{:S(2)}, u32[]{:S(2)}) async-start(bf16[64,32,176]{2,0,1:T(8,128)(2,1)} %copy.21), calls=%async_computation | async-start | bytes 2097152 | tf_op jit(solution)/shard_map/all_to_all | solution.py:52
  51.2 14.4 %all_gather.22 = bf16[64,5632]{1,0:T(8,128)(2,1)S(1)} all-gather(bf16[64,1408]{1,0:T(8,128)(2,1)S(1)} %convert_element_type.63), channel_id=1, replica_groups=mesh['grp'=2,'fs_0'=16,'fs_1'=2,'tp'=4] {'tp'}, dimensions={1}, use_global_device_ids=true | all-gather | bytes 901120 | tf_op jit(solution)/shard_map/all_gather | solution.py:48
  69.1 37.3 %all-to-all-done = bf16[64,32,176]{2,0,1:T(8,128)(2,1)S(1)} async-done(((bf16[64,32,176]{2,0,1:T(8,128)(2,1)}), bf16[64,32,176]{2,0,1:T(8,128)(2,1)S(1)}, u32[]{:S(2)}, u32[]{:S(2)}) %all-to-all-start) | async-done | bytes 720928 | tf_op jit(solution)/shard_map/all_to_all | solution.py:52
  106.4 4.8 all-to-all-start.1
  111.4 14.2 %all_gather.23 = bf16[176,2048]{1,0:T(8,128)(2,1)S(1)} all-gather(bf16[176,512]{1,0:T(8,128)(2,1)S(1)} %convert_element_type.65), channel_id=1, replica_groups=mesh['grp'=2,'fs_0'=16,'fs_1'=2,'tp'=4] {'tp'}, dimensions={1}, use_global_device_ids=true | all-gather | bytes 901120 | tf_op jit(solution)/shard_map/all_gather | solution.py:49
  125.6 4.0 fusion.2
  129.6 37.3 %all-to-all-done.1 = bf16[64,32,176]{2,0,1:T(8,128)(2,1)S(1)} async-done(((bf16[64,32,176]{2,0,1:T(8,128)(2,1)}), bf16[64,32,176]{2,0,1:T(8,128)(2,1)S(1)}, u32[]{:S(2)}, u32[]{:S(2)}) %all-to-all-start.1) | async-done | bytes 720928 | tf_op jit(solution)/shard_map/all_to_all | solution.py:53
  167.0 7.0 %convolution_convert_fusion.1 = bf16[1024,2048]{1,0:T(8,128)(2,1)} fusion(bf16[176,2048]{1,0:T(8,128)(2,1)S(1)} %all_gather.23, bf16[2048,176]{1,0:T(8,128)(2,1)S(1)} %bitcast.57, bf16[1,1024,2048]{2,1,0:T(8,128)(2,1)} %param.8, f32[1024,176]{0,1:T(8,128)S(1)} %fusion.2), kind=kOutput, calls=%fused_computation.5 | convolution fusion | flops 1479573504 | bytes 10551296 | tf_op jit(solution)/shard_map/dot_general | solution.py:59
  173.9 4.7 copy.23
  178.8 12.5 %reduce-scatter.5.cloned.1.call-done = bf16[16,32,2048]{2,1,0:T(8,128)(2,1)} async-done(((bf16[32,32,2048]{2,1,0:T(8,128)(2,1)}), bf16[16,32,2048]{2,1,0:T(8,128)(2,1)}) %reduce-scatter.5.cloned.1.call-update) | async-done | bytes 2097168 | tf_op jit(solution)/shard_map/reduce_scatter | solution.py:18
  191.4 75.9 %reduce-scatter.7.cloned.1.call-done = bf16[1,32,2048]{2,1,0:T(8,128)(2,1)} async-done(((bf16[16,32,2048]{2,1,0:T(8,128)(2,1)}), bf16[1,32,2048]{2,1,0:T(8,128)(2,1)}) %reduce-scatter.7.cloned.1.call-update) | async-done | bytes 131088 | tf_op jit(solution)/shard_map/reduce_scatter | solution.py:18
  271.7 14.1 %all_gather.25 = bf16[64,5632]{1,0:T(8,128)(2,1)} all-gather(bf16[64,1408]{1,0:T(8,128)(2,1)S(1)} %get-tuple-element.14), channel_id=1, replica_groups=mesh['grp'=2,'fs_0'=16,'fs_1'=2,'tp'=4] {'tp'}, dimensions={1}, use_global_device_ids=true | all-gather | bytes 901120 | tf_op jit(solution)/shard_map/all_gather | solution.py:47
  290.4 9.7 %all-to-all-start.2 = ((bf16[64,32,176]{2,0,1:T(8,128)(2,1)}), bf16[64,32,176]{2,0,1:T(8,128)(2,1)S(1)}, u32[]{:S(2)}, u32[]{:S(2)}) async-start(bf16[64,32,176]{2,0,1:T(8,128)(2,1)} %copy.24), calls=%async_computation.4 | async-start | bytes 2097152 | tf_op jit(solution)/shard_map/all_to_all | solution.py:52
  300.1 14.3 %all_gather.26 = bf16[64,5632]{1,0:T(8,128)(2,1)} all-gather(bf16[64,1408]{1,0:T(8,128)(2,1)S(1)} %get-tuple-element.15), channel_id=1, replica_groups=mesh['grp'=2,'fs_0'=16,'fs_1'=2,'tp'=4] {'tp'}, dimensions={1}, use_global_device_ids=true | all-gather | bytes 901120 | tf_op jit(solution)/shard_map/all_gather | solution.py:48
  321.0 44.7 %all-to-all-done.2 = bf16[64,32,176]{2,0,1:T(8,128)(2,1)S(1)} async-done(((bf16[64,32,176]{2,0,1:T(8,128)(2,1)}), bf16[64,32,176]{2,0,1:T(8,128)(2,1)S(1)}, u32[]{:S(2)}, u32[]{:S(2)}) %all-to-all-start.2) | async-done | bytes 720928 | tf_op jit(solution)/shard_map/all_to_all | solution.py:52
  365.7 5.7 %all-to-all-start.3 = ((bf16[64,32,176]{2,0,1:T(8,128)(2,1)}), bf16[64,32,176]{2,0,1:T(8,128)(2,1)}, u32[]{:S(2)}, u32[]{:S(2)}) async-start(bf16[64,32,176]{2,0,1:T(8,128)(2,1)} %copy.25), calls=%async_computation.5 | async-start | bytes 2097152 | tf_op jit(solution)/shard_map/all_to_all | solution.py:53
  371.5 14.5 %all_gather.27 = bf16[176,2048]{1,0:T(8,128)(2,1)} all-gather(bf16[176,512]{1,0:T(8,128)(2,1)S(1)} %convert_element_type.74), channel_id=1, replica_groups=mesh['grp'=2,'fs_0'=16,'fs_1'=2,'tp'=4] {'tp'}, dimensions={1}, use_global_device_ids=true | all-gather | bytes 901120 | tf_op jit(solution)/shard_map/all_gather | solution.py:49
  386.0 4.6 fusion.29
  390.6 36.6 %all-to-all-done.3 = bf16[64,32,176]{2,0,1:T(8,128)(2,1)} async-done(((bf16[64,32,176]{2,0,1:T(8,128)(2,1)}), bf16[64,32,176]{2,0,1:T(8,128)(2,1)}, u32[]{:S(2)}, u32[]{:S(2)}) %all-to-all-start.3) | async-done | bytes 720928 | tf_op jit(solution)/shard_map/all_to_all | solution.py:53
  427.2 7.7 %convolution_convert_fusion = bf16[1024,2048]{1,0:T(8,128)(2,1)} fusion(bf16[176,2048]{1,0:T(8,128)(2,1)} %all_gather.27, bf16[1024,2048]{1,0:T(8,128)(2,1)} %all-gather.2.cloned.1.call-done, bf16[2048,176]{1,0:T(8,128)(2,1)} %bitcast.12, f32[1024,176]{0,1:T(8,128)} %fusion.29), kind=kOutput, calls=%fused_computation.4 | convolution fusion | flops 1479573504 | bytes 10551296 | tf_op jit(solution)/shard_map/dot_general | solution.py:59
  434.9 4.7 copy.26
  439.7 11.8 %reduce-scatter.9.cloned.1.call-done = bf16[16,32,2048]{2,1,0:T(8,128)(2,1)} async-done(((bf16[32,32,2048]{2,1,0:T(8,128)(2,1)}), bf16[16,32,2048]{2,1,0:T(8,128)(2,1)}) %reduce-scatter.9.cloned.1.call-update) | async-done | bytes 2097168 | tf_op jit(solution)/shard_map/reduce_scatter | solution.py:18
  457.6 70.1 %reduce-scatter.11.cloned.1.call-done = bf16[1,32,2048]{2,1,0:T(8,128)(2,1)} async-done(((bf16[16,32,2048]{2,1,0:T(8,128)(2,1)}), bf16[1,32,2048]{2,1,0:T(8,128)(2,1)}) %reduce-scatter.11.cloned.1.call-update) | async-done | bytes 131088 | tf_op jit(solution)/shard_map/reduce_scatter | solution.py:18
  (60 shorter events, 36.2 us)
Async XLA Ops:
  7.2 43.9 %copy-start.3 = (f32[64,1408]{1,0:T(8,128)S(1)}, f32[64,1408]{1,0:T(8,128)}, u32[]{:S(2)}) copy-start(f32[64,1408]{1,0:T(8,128)} %param.10) | copy-start | bytes 1081348
  41.4 65.0 %all-to-all-start = ((bf16[64,32,176]{2,0,1:T(8,128)(2,1)}), bf16[64,32,176]{2,0,1:T(8,128)(2,1)S(1)}, u32[]{:S(2)}, u32[]{:S(2)}) async-start(bf16[64,32,176]{2,0,1:T(8,128)(2,1)} %copy.21), calls=%async_computation | async-start | bytes 2097152 | tf_op jit(solution)/shard_map/all_to_all | solution.py:52
  51.1 60.2 %copy-start.4 = (f32[176,512]{1,0:T(8,128)S(1)}, f32[176,512]{1,0:T(8,128)}, u32[]{:S(2)}) copy-start(f32[176,512]{1,0:T(8,128)} %param.11) | copy-start | bytes 1081348
  106.4 60.6 %all-to-all-start.1 = ((bf16[64,32,176]{2,0,1:T(8,128)(2,1)}), bf16[64,32,176]{2,0,1:T(8,128)(2,1)S(1)}, u32[]{:S(2)}, u32[]{:S(2)}) async-start(bf16[64,32,176]{2,0,1:T(8,128)(2,1)} %copy.22), calls=%async_computation.1 | async-start | bytes 2097152 | tf_op jit(solution)/shard_map/all_to_all | solution.py:53
  111.3 80.0 %reduce-scatter.5.cloned.1.call-start = ((), (), s32[]{:S(2)}) async-start(), calls=%async_computation.8 | async-start | bytes 6291456 | tf_op jit(solution)/shard_map/reduce_scatter | solution.py:18
  125.6 41.4 %copy-start = (bf16[176,2048]{1,0:T(8,128)(2,1)}, bf16[176,2048]{1,0:T(8,128)(2,1)S(1)}, u32[]{:S(2)}) copy-start(bf16[176,2048]{1,0:T(8,128)(2,1)S(1)} %all_gather.23) | copy-start | bytes 2162692
  178.7 92.8 %copy-start.8 = (f32[2048]{0:T(1024)S(1)}, f32[2048]{0:T(1024)}, u32[]{:S(2)}) copy-start(f32[2048]{0:T(1024)} %param.12) | copy-start | bytes 24580
  178.7 92.9 %copy-start.6 = (f32[64,1408]{1,0:T(8,128)S(1)}, f32[64,1408]{1,0:T(8,128)}, u32[]{:S(2)}) copy-start(f32[64,1408]{1,0:T(8,128)} %param.13) | copy-start | bytes 1081348
  178.7 92.9 %copy-start.7 = (f32[64,1408]{1,0:T(8,128)S(1)}, f32[64,1408]{1,0:T(8,128)}, u32[]{:S(2)}) copy-start(f32[64,1408]{1,0:T(8,128)} %param.14) | copy-start | bytes 1081348
  178.7 88.6 %reduce-scatter.7.cloned.1.call-start = ((), (), s32[]{:S(2)}) async-start(), calls=%async_computation.9 | async-start | bytes 2228224 | tf_op jit(solution)/shard_map/reduce_scatter | solution.py:18
  191.3 194.7 %all-gather.2.cloned.1.call-start = ((), (), s32[]{:S(2)}) async-start(), calls=%async_computation.10 | async-start | bytes 4325376 | tf_op jit(solution)/shard_map/all_gather | solution.py:87
  290.4 75.3 %all-to-all-start.2 = ((bf16[64,32,176]{2,0,1:T(8,128)(2,1)}), bf16[64,32,176]{2,0,1:T(8,128)(2,1)S(1)}, u32[]{:S(2)}, u32[]{:S(2)}) async-start(bf16[64,32,176]{2,0,1:T(8,128)(2,1)} %copy.24), calls=%async_computation.4 | async-start | bytes 2097152 | tf_op jit(solution)/shard_map/all_to_all | solution.py:52
  314.4 57.1 %copy-start.5 = (f32[176,512]{1,0:T(8,128)S(1)}, f32[176,512]{1,0:T(8,128)}, u32[]{:S(2)}) copy-start(f32[176,512]{1,0:T(8,128)} %param.15) | copy-start | bytes 1081348
  365.7 61.5 %all-to-all-start.3 = ((bf16[64,32,176]{2,0,1:T(8,128)(2,1)}), bf16[64,32,176]{2,0,1:T(8,128)(2,1)}, u32[]{:S(2)}, u32[]{:S(2)}) async-start(bf16[64,32,176]{2,0,1:T(8,128)(2,1)} %copy.25), calls=%async_computation.5 | async-start | bytes 2097152 | tf_op jit(solution)/shard_map/all_to_all | solution.py:53
  371.4 80.1 %reduce-scatter.9.cloned.1.call-start = ((), (), s32[]{:S(2)}) async-start(), calls=%async_computation.11 | async-start | bytes 6291456 | tf_op jit(solution)/shard_map/reduce_scatter | solution.py:18
  439.7 87.9 %reduce-scatter.11.cloned.1.call-start = ((), (), s32[]{:S(2)}) async-start(), calls=%async_computation.12 | async-start | bytes 2228224 | tf_op jit(solution)/shard_map/reduce_scatter | solution.py:18
  452.9 78.9 %copy-start.1 = (bf16[176,2048]{1,0:T(8,128)(2,1)S(1)}, bf16[176,2048]{1,0:T(8,128)(2,1)}, u32[]{:S(2)}) copy-start(bf16[176,2048]{1,0:T(8,128)(2,1)} %copy-done) | copy-start | bytes 2162692
  452.9 79.8 %copy-start.2 = (bf16[176,2048]{1,0:T(8,128)(2,1)S(1)}, bf16[176,2048]{1,0:T(8,128)(2,1)}, u32[]{:S(2)}) copy-start(bf16[176,2048]{1,0:T(8,128)(2,1)} %all_gather.27) | copy-start | bytes 2162692
Sparse Core Ops, SparseCore 0:
  178.9 12.3 reduce-scatter.4
  193.8 73.4 reduce-scatter.6
  271.6 98.2 all-gather.1
  439.8 11.7 reduce-scatter.8
  454.0 73.5 reduce-scatter.10
where the time goes:
time: 541 us; the launch traced here: 540 us
  waiting for transfers between devices  326 us (60%)
  blocking collectives  101 us (19%)
  local copies, waits for them, and re-layouts  35.6 us (7%)
  starting transfers between devices  30.2 us (6%)
  matrix products  23.2 us (4%)
  between operations  14 us (3%)
  other arithmetic  9.45 us (2%)
    reduce_scatter x4, waiting for transfers between devices, reduced_to_own(): pieces = lax.psum_scatter(pieces, axes[k], scatter_dimension=0, tiled=True)  170 us
    all_to_all x2, waiting for transfers between devices, relay_weights(): lax.all_to_all(gate_rows, FS, split_axis=1, concat_axis=0, tiled=True)  82 us
    all_to_all x2, waiting for transfers between devices, relay_weights(): lax.all_to_all(up_rows, FS, split_axis=1, concat_axis=0, tiled=True)  73.9 us
    all_gather x2, blocking collectives, relay_weights(): lax.all_gather(gate_proj, 'tp', axis=1, tiled=True)  43.7 us
    all_gather x2, blocking collectives, relay_weights(): lax.all_gather(down_proj, 'tp', axis=1, tiled=True)  28.7 us
    all_gather x2, blocking collectives, relay_weights(): lax.all_gather(up_proj, 'tp', axis=1, tiled=True)  28.6 us
    all_to_all x2, starting transfers between devices, relay_weights(): lax.all_to_all(gate_rows, FS, split_axis=1, concat_axis=0, tiled=True)  19.4 us
    dot_general x2, matrix products, row_terms(): return jnp.dot(hidden, down_proj, preferred_element_type=jnp.float32)  14.6 us
  transfers between devices with their start and end apart: 9, of which 8 were waited for; matrix products, arithmetic and copies ran while one was open for 4% of the time, Pallas kernels for 0%

commit v1 on v0

--- a/solution.py
+++ b/solution.py
@@ -8,6 +8,12 @@
 norm_eps = 1e-05
 deep_alpha = 2.0**0.25
 half_step = 0.5
+
+
+def stack_and_merge(x, axis, dim):
+    parts = lax.all_gather(x, axis, axis=0, tiled=False)
+    result = jnp.concatenate(parts, axis=dim)
+    return result
 
 
 def reduced_to_own(pieces, axes, sequence):
@@ -44,7 +50,7 @@
 
 def relay_weights(gate_proj, up_proj, down_proj):
     gate_rows, up_rows, down_mine = (
-        lax.all_gather(gate_proj, "tp", axis=1, tiled=True),
+        stack_and_merge(gate_proj, "tp", 1),
         lax.all_gather(up_proj, "tp", axis=1, tiled=True),
         lax.all_gather(down_proj, "tp", axis=1, tiled=True),
     )

time: 541 us -> 541 us (level)
  no operation moved by 1% of the time
where the time goes in v1:
time: 541 us; the launch traced here: 540 us
  waiting for transfers between devices  326 us (60%)
  blocking collectives  100 us (18%)
  local copies, waits for them, and re-layouts  36.8 us (7%)
  starting transfers between devices  30.2 us (6%)
  matrix products  23.2 us (4%)
  between operations  14 us (3%)
  other arithmetic  9.4 us (2%)
    reduce_scatter x4, waiting for transfers between devices, reduced_to_own(): pieces = lax.psum_scatter(pieces, axes[k], scatter_dimension=0, tiled=True)  170 us
    all_to_all x2, waiting for transfers between devices, relay_weights(): lax.all_to_all(gate_rows, FS, split_axis=1, concat_axis=0, tiled=True)  81.6 us
    all_to_all x2, waiting for transfers between devices, relay_weights(): lax.all_to_all(up_rows, FS, split_axis=1, concat_axis=0, tiled=True)  74.2 us
    all_gather x2, blocking collectives, stack_and_merge(): parts = lax.all_gather(x, axis, axis=0, tiled=False)  42.8 us
    all_gather x2, blocking collectives, relay_weights(): lax.all_gather(up_proj, 'tp', axis=1, tiled=True)  28.8 us
    all_gather x2, blocking collectives, relay_weights(): lax.all_gather(down_proj, 'tp', axis=1, tiled=True)  28.4 us
    all_to_all x2, starting transfers between devices, relay_weights(): lax.all_to_all(gate_rows, FS, split_axis=1, concat_axis=0, tiled=True)  19.4 us
    dot_general x2, matrix products, row_terms(): return jnp.dot(hidden, down_proj, preferred_element_type=jnp.float32)  14.6 us
  transfers between devices with their start and end apart: 9, of which 8 were waited for; matrix products, arithmetic and copies ran while one was open for 4% of the time, Pallas kernels for 0%

profile of v1, /device:TPU:34, one launch (start us, length us, event | category | flops | bytes accessed | tf_op | source)
XLA Modules:
  0.0 540.1 jit_solution(3214939865761774351)
XLA Ops:
  8.2 29.6 %all-gather = bf16[256,1408]{1,0:T(8,128)(2,1)S(1)} all-gather(bf16[64,1408]{1,0:T(8,128)(2,1)S(1)} %convert_element_type.62), channel_id=2, replica_groups=mesh['grp'=2,'fs_0'=16,'fs_1'=2,'tp'=4] {'tp'}, dimensions={0}, use_global_device_ids=true | all-gather | bytes 901120 | tf_op jit(solution)/shard_map/all_gather | solution.py:14
  41.5 9.6 %all-to-all-start = ((bf16[64,32,176]{2,0,1:T(8,128)(2,1)}), bf16[64,32,176]{2,0,1:T(8,128)(2,1)S(1)}, u32[]{:S(2)}, u32[]{:S(2)}) async-start(bf16[64,32,176]{2,0,1:T(8,128)(2,1)} %copy.32), calls=%async_computation | async-start | bytes 2097152 | tf_op jit(solution)/shard_map/all_to_all | solution.py:58
  51.2 14.4 %all_gather.29 = bf16[64,5632]{1,0:T(8,128)(2,1)S(1)} all-gather(bf16[64,1408]{1,0:T(8,128)(2,1)S(1)} %convert_element_type.63), channel_id=1, replica_groups=mesh['grp'=2,'fs_0'=16,'fs_1'=2,'tp'=4] {'tp'}, dimensions={1}, use_global_device_ids=true | all-gather | bytes 901120 | tf_op jit(solution)/shard_map/all_gather | solution.py:54
  69.2 37.2 %all-to-all-done = bf16[64,32,176]{2,0,1:T(8,128)(2,1)S(1)} async-done(((bf16[64,32,176]{2,0,1:T(8,128)(2,1)}), bf16[64,32,176]{2,0,1:T(8,128)(2,1)S(1)}, u32[]{:S(2)}, u32[]{:S(2)}) %all-to-all-start) | async-done | bytes 720928 | tf_op jit(solution)/shard_map/all_to_all | solution.py:58
  106.4 4.8 all-to-all-start.1
  111.4 14.3 %all_gather.30 = bf16[176,2048]{1,0:T(8,128)(2,1)S(1)} all-gather(bf16[176,512]{1,0:T(8,128)(2,1)S(1)} %convert_element_type.65), channel_id=1, replica_groups=mesh['grp'=2,'fs_0'=16,'fs_1'=2,'tp'=4] {'tp'}, dimensions={1}, use_global_device_ids=true | all-gather | bytes 901120 | tf_op jit(solution)/shard_map/all_gather | solution.py:55
  125.7 4.0 fusion.2
  129.7 37.3 %all-to-all-done.1 = bf16[64,32,176]{2,0,1:T(8,128)(2,1)S(1)} async-done(((bf16[64,32,176]{2,0,1:T(8,128)(2,1)}), bf16[64,32,176]{2,0,1:T(8,128)(2,1)S(1)}, u32[]{:S(2)}, u32[]{:S(2)}) %all-to-all-start.1) | async-done | bytes 720928 | tf_op jit(solution)/shard_map/all_to_all | solution.py:59
  167.0 7.0 %convolution_convert_fusion.1 = bf16[1024,2048]{1,0:T(8,128)(2,1)} fusion(bf16[176,2048]{1,0:T(8,128)(2,1)S(1)} %all_gather.30, bf16[2048,176]{1,0:T(8,128)(2,1)S(1)} %bitcast.65, bf16[1,1024,2048]{2,1,0:T(8,128)(2,1)} %param.8, f32[1024,176]{0,1:T(8,128)S(1)} %fusion.2), kind=kOutput, calls=%fused_computation.5 | convolution fusion | flops 1479573504 | bytes 10551296 | tf_op jit(solution)/shard_map/dot_general | solution.py:65
  173.9 4.7 copy.34
  178.8 12.5 %reduce-scatter.5.cloned.1.call-done = bf16[16,32,2048]{2,1,0:T(8,128)(2,1)} async-done(((bf16[32,32,2048]{2,1,0:T(8,128)(2,1)}), bf16[16,32,2048]{2,1,0:T(8,128)(2,1)}) %reduce-scatter.5.cloned.1.call-update) | async-done | bytes 2097168 | tf_op jit(solution)/shard_map/reduce_scatter | solution.py:24
  191.4 76.0 %reduce-scatter.7.cloned.1.call-done = bf16[1,32,2048]{2,1,0:T(8,128)(2,1)} async-done(((bf16[16,32,2048]{2,1,0:T(8,128)(2,1)}), bf16[1,32,2048]{2,1,0:T(8,128)(2,1)}) %reduce-scatter.7.cloned.1.call-update) | async-done | bytes 131088 | tf_op jit(solution)/shard_map/reduce_scatter | solution.py:24
  271.7 13.2 %all-gather.1 = bf16[256,1408]{1,0:T(8,128)(2,1)S(1)} all-gather(bf16[64,1408]{1,0:T(8,128)(2,1)S(1)} %get-tuple-element.21), channel_id=3, replica_groups=mesh['grp'=2,'fs_0'=16,'fs_1'=2,'tp'=4] {'tp'}, dimensions={0}, use_global_device_ids=true | all-gather | bytes 901120 | tf_op jit(solution)/shard_map/all_gather | solution.py:14
  290.7 9.8 %all-to-all-start.2 = ((bf16[64,32,176]{2,0,1:T(8,128)(2,1)}), bf16[64,32,176]{2,0,1:T(8,128)(2,1)S(1)}, u32[]{:S(2)}, u32[]{:S(2)}) async-start(bf16[64,32,176]{2,0,1:T(8,128)(2,1)} %copy.36), calls=%async_computation.4 | async-start | bytes 2097152 | tf_op jit(solution)/shard_map/all_to_all | solution.py:58
  300.5 14.4 %all_gather.34 = bf16[64,5632]{1,0:T(8,128)(2,1)} all-gather(bf16[64,1408]{1,0:T(8,128)(2,1)S(1)} %get-tuple-element.22), channel_id=1, replica_groups=mesh['grp'=2,'fs_0'=16,'fs_1'=2,'tp'=4] {'tp'}, dimensions={1}, use_global_device_ids=true | all-gather | bytes 901120 | tf_op jit(solution)/shard_map/all_gather | solution.py:54
  321.5 44.4 %all-to-all-done.2 = bf16[64,32,176]{2,0,1:T(8,128)(2,1)S(1)} async-done(((bf16[64,32,176]{2,0,1:T(8,128)(2,1)}), bf16[64,32,176]{2,0,1:T(8,128)(2,1)S(1)}, u32[]{:S(2)}, u32[]{:S(2)}) %all-to-all-start.2) | async-done | bytes 720928 | tf_op jit(solution)/shard_map/all_to_all | solution.py:58
  365.9 5.7 %all-to-all-start.3 = ((bf16[64,32,176]{2,0,1:T(8,128)(2,1)}), bf16[64,32,176]{2,0,1:T(8,128)(2,1)}, u32[]{:S(2)}, u32[]{:S(2)}) async-start(bf16[64,32,176]{2,0,1:T(8,128)(2,1)} %copy.37), calls=%async_computation.5 | async-start | bytes 2097152 | tf_op jit(solution)/shard_map/all_to_all | solution.py:59
  371.7 14.2 %all_gather.35 = bf16[176,2048]{1,0:T(8,128)(2,1)} all-gather(bf16[176,512]{1,0:T(8,128)(2,1)S(1)} %convert_element_type.74), channel_id=1, replica_groups=mesh['grp'=2,'fs_0'=16,'fs_1'=2,'tp'=4] {'tp'}, dimensions={1}, use_global_device_ids=true | all-gather | bytes 901120 | tf_op jit(solution)/shard_map/all_gather | solution.py:55
  385.9 4.6 fusion.29
  390.5 36.9 %all-to-all-done.3 = bf16[64,32,176]{2,0,1:T(8,128)(2,1)} async-done(((bf16[64,32,176]{2,0,1:T(8,128)(2,1)}), bf16[64,32,176]{2,0,1:T(8,128)(2,1)}, u32[]{:S(2)}, u32[]{:S(2)}) %all-to-all-start.3) | async-done | bytes 720928 | tf_op jit(solution)/shard_map/all_to_all | solution.py:59
  427.4 7.7 %convolution_convert_fusion = bf16[1024,2048]{1,0:T(8,128)(2,1)} fusion(bf16[176,2048]{1,0:T(8,128)(2,1)} %all_gather.35, bf16[1024,2048]{1,0:T(8,128)(2,1)} %all-gather.4.cloned.1.call-done, bf16[2048,176]{1,0:T(8,128)(2,1)} %bitcast.16, f32[1024,176]{0,1:T(8,128)} %fusion.29), kind=kOutput, calls=%fused_computation.4 | convolution fusion | flops 1479573504 | bytes 10551296 | tf_op jit(solution)/shard_map/dot_general | solution.py:65
  435.1 4.7 copy.38
  439.9 11.9 %reduce-scatter.9.cloned.1.call-done = bf16[16,32,2048]{2,1,0:T(8,128)(2,1)} async-done(((bf16[32,32,2048]{2,1,0:T(8,128)(2,1)}), bf16[16,32,2048]{2,1,0:T(8,128)(2,1)}) %reduce-scatter.9.cloned.1.call-update) | async-done | bytes 2097168 | tf_op jit(solution)/shard_map/reduce_scatter | solution.py:24
  457.8 69.9 %reduce-scatter.11.cloned.1.call-done = bf16[1,32,2048]{2,1,0:T(8,128)(2,1)} async-done(((bf16[16,32,2048]{2,1,0:T(8,128)(2,1)}), bf16[1,32,2048]{2,1,0:T(8,128)(2,1)}) %reduce-scatter.11.cloned.1.call-update) | async-done | bytes 131088 | tf_op jit(solution)/shard_map/reduce_scatter | solution.py:24
  (62 shorter events, 37.3 us)
Async XLA Ops:
  8.2 42.9 %copy-start.3 = (f32[64,1408]{1,0:T(8,128)S(1)}, f32[64,1408]{1,0:T(8,128)}, u32[]{:S(2)}) copy-start(f32[64,1408]{1,0:T(8,128)} %param.10) | copy-start | bytes 1081348
  41.5 64.9 %all-to-all-start = ((bf16[64,32,176]{2,0,1:T(8,128)(2,1)}), bf16[64,32,176]{2,0,1:T(8,128)(2,1)S(1)}, u32[]{:S(2)}, u32[]{:S(2)}) async-start(bf16[64,32,176]{2,0,1:T(8,128)(2,1)} %copy.32), calls=%async_computation | async-start | bytes 2097152 | tf_op jit(solution)/shard_map/all_to_all | solution.py:58
  51.1 60.2 %copy-start.4 = (f32[176,512]{1,0:T(8,128)S(1)}, f32[176,512]{1,0:T(8,128)}, u32[]{:S(2)}) copy-start(f32[176,512]{1,0:T(8,128)} %param.11) | copy-start | bytes 1081348
  106.4 60.6 %all-to-all-start.1 = ((bf16[64,32,176]{2,0,1:T(8,128)(2,1)}), bf16[64,32,176]{2,0,1:T(8,128)(2,1)S(1)}, u32[]{:S(2)}, u32[]{:S(2)}) async-start(bf16[64,32,176]{2,0,1:T(8,128)(2,1)} %copy.33), calls=%async_computation.1 | async-start | bytes 2097152 | tf_op jit(solution)/shard_map/all_to_all | solution.py:59
  111.3 80.0 %reduce-scatter.5.cloned.1.call-start = ((), (), s32[]{:S(2)}) async-start(), calls=%async_computation.8 | async-start | bytes 6291456 | tf_op jit(solution)/shard_map/reduce_scatter | solution.py:24
  125.7 41.3 %copy-start = (bf16[176,2048]{1,0:T(8,128)(2,1)}, bf16[176,2048]{1,0:T(8,128)(2,1)S(1)}, u32[]{:S(2)}) copy-start(bf16[176,2048]{1,0:T(8,128)(2,1)S(1)} %all_gather.30) | copy-start | bytes 2162692
  178.7 92.9 %copy-start.8 = (f32[2048]{0:T(1024)S(1)}, f32[2048]{0:T(1024)}, u32[]{:S(2)}) copy-start(f32[2048]{0:T(1024)} %param.12) | copy-start | bytes 24580
  178.7 93.0 %copy-start.6 = (f32[64,1408]{1,0:T(8,128)S(1)}, f32[64,1408]{1,0:T(8,128)}, u32[]{:S(2)}) copy-start(f32[64,1408]{1,0:T(8,128)} %param.13) | copy-start | bytes 1081348
  178.7 93.0 %copy-start.7 = (f32[64,1408]{1,0:T(8,128)S(1)}, f32[64,1408]{1,0:T(8,128)}, u32[]{:S(2)}) copy-start(f32[64,1408]{1,0:T(8,128)} %param.14) | copy-start | bytes 1081348
  178.7 88.7 %reduce-scatter.7.cloned.1.call-start = ((), (), s32[]{:S(2)}) async-start(), calls=%async_computation.9 | async-start | bytes 2228224 | tf_op jit(solution)/shard_map/reduce_scatter | solution.py:24
  191.4 194.5 %all-gather.4.cloned.1.call-start = ((), (), s32[]{:S(2)}) async-start(), calls=%async_computation.10 | async-start | bytes 4325376 | tf_op jit(solution)/shard_map/all_gather | solution.py:93
  290.7 75.2 %all-to-all-start.2 = ((bf16[64,32,176]{2,0,1:T(8,128)(2,1)}), bf16[64,32,176]{2,0,1:T(8,128)(2,1)S(1)}, u32[]{:S(2)}, u32[]{:S(2)}) async-start(bf16[64,32,176]{2,0,1:T(8,128)(2,1)} %copy.36), calls=%async_computation.4 | async-start | bytes 2097152 | tf_op jit(solution)/shard_map/all_to_all | solution.py:58
  314.9 56.8 %copy-start.5 = (f32[176,512]{1,0:T(8,128)S(1)}, f32[176,512]{1,0:T(8,128)}, u32[]{:S(2)}) copy-start(f32[176,512]{1,0:T(8,128)} %param.15) | copy-start | bytes 1081348
  365.9 61.5 %all-to-all-start.3 = ((bf16[64,32,176]{2,0,1:T(8,128)(2,1)}), bf16[64,32,176]{2,0,1:T(8,128)(2,1)}, u32[]{:S(2)}, u32[]{:S(2)}) async-start(bf16[64,32,176]{2,0,1:T(8,128)(2,1)} %copy.37), calls=%async_computation.5 | async-start | bytes 2097152 | tf_op jit(solution)/shard_map/all_to_all | solution.py:59
  371.6 80.2 %reduce-scatter.9.cloned.1.call-start = ((), (), s32[]{:S(2)}) async-start(), calls=%async_computation.11 | async-start | bytes 6291456 | tf_op jit(solution)/shard_map/reduce_scatter | solution.py:24
  439.8 87.8 %reduce-scatter.11.cloned.1.call-start = ((), (), s32[]{:S(2)}) async-start(), calls=%async_computation.12 | async-start | bytes 2228224 | tf_op jit(solution)/shard_map/reduce_scatter | solution.py:24
  453.1 78.8 %copy-start.1 = (bf16[176,2048]{1,0:T(8,128)(2,1)S(1)}, bf16[176,2048]{1,0:T(8,128)(2,1)}, u32[]{:S(2)}) copy-start(bf16[176,2048]{1,0:T(8,128)(2,1)} %copy-done) | copy-start | bytes 2162692
  453.1 79.6 %copy-start.2 = (bf16[176,2048]{1,0:T(8,128)(2,1)S(1)}, bf16[176,2048]{1,0:T(8,128)(2,1)}, u32[]{:S(2)}) copy-start(bf16[176,2048]{1,0:T(8,128)(2,1)} %all_gather.35) | copy-start | bytes 2162692
Sparse Core Ops, SparseCore 0:
  178.8 12.3 reduce-scatter.4
  193.8 73.5 reduce-scatter.6
  271.7 98.3 all-gather.3
  440.0 11.7 reduce-scatter.8
  454.2 73.4 reduce-scatter.10
